TPU v7x, 32 devices: a whole 2x2x4 slice. The times are simulated.
32 devices in a mesh: sp: 8 (over z, y), tp: 4 (over x, core).
Axes of the slice: x: 2, y: 2, z: 4, core: 2. Of those that a mesh axis runs over, the one named last changes fastest.
Arguments:
- out_grad: bfloat16 [2048, 4096], P('sp'), may hold values from -6 to 6
- stream: bfloat16 [2048, 4096], P('sp'), may hold values from -6 to 6
- norm_gain: bfloat16 [4096], replicated, may hold values from 0.099609375 to 1.8984375
- routes: int32 [2048, 2], P('sp'), may hold values from 0 to 7, all different within a row; in each aligned block of 256 rows (0 to 255, 256 to 511, ...) at most 80 rows name the same one
- route_weight: float32 [2048, 2], P('sp'), may hold values from 0.3 to 1.5
- gate_weight: bfloat16 [8, 4096, 1024], P('sp', None, 'tp'), may hold values from -0.09375 to 0.09375
- up_weight: bfloat16 [8, 4096, 1024], P('sp', None, 'tp'), may hold values from -0.09375 to 0.09375
- down_weight: bfloat16 [8, 1024, 4096], P('sp', 'tp'), may hold values from -0.1875 to 0.1875
- out_proj: bfloat16 [4096, 1024], P(None, 'tp'), may hold values from -0.1875 to 0.1875
- conv_out: bfloat16 [2048, 1024], P('sp', 'tp'), as said below
- gate_branch: bfloat16 [2048, 1024], P('sp', 'tp'), may hold values from -6 to 6
- decay_map: bfloat16 [2, 4, 256, 256], P(None, 'tp'), as said below
- input_map: bfloat16 [2, 4, 256, 256], P(None, 'tp'), as said below
- decay_param: float32 [2, 1024], P(None, 'tp'), as said below
- decay_shift: float32 [2, 2048, 1024], P(None, 'sp', 'tp'), as said below
- states: float32 [2, 2048, 1024], P(None, 'sp', 'tp'), as said below
Outputs:
- conv_grad: float32 [2048, 1024], P('sp', 'tp')
- gate_branch_grad: float32 [2048, 1024], P('sp', 'tp')
- out_proj_grad: float32 [4096, 1024], P('sp', 'tp')
- gate_weight_grad: bfloat16 [8, 4096, 1024], P('sp', None, 'tp')
- up_weight_grad: bfloat16 [8, 4096, 1024], P('sp', None, 'tp')
- down_weight_grad: bfloat16 [8, 1024, 4096], P('sp', 'tp')
Inputs may be any that keep to these rules, and one draw needn't show every extreme that they name: `routes`: each token names 2 different experts. Among the 256 tokens of one index of sp no expert is named more than 80 times, a bound that some expert reaches in some of these blocks. `conv_out`: within -6 to 6. `decay_map`: entries within -4 to 4 times 256 to the power -0.5. `input_map`: entries within -4 to 4 times 256 to the power -0.5. `decay_param`: between 3.7 and 3.5 plus the logarithm of 2048. `decay_shift`: every entry lies between -0.7 and -0.00002. The forward pass's states: they follow the recurrences of the steps from conv_out, decay_map, input_map, decay_param and decay_shift.
All inputs are finite; a program needn't handle non-finite values.
Results may differ from a plain program's by a relative error of at most 0.018.
Values may be sent and summed in bfloat16 or wider, within the bound.
A program may use at most 128 MiB of HBM per device.

v0:
```python
import jax
import jax.numpy as jnp
from jax import lax
from jax.sharding import PartitionSpec as P

TOP = 2
EXP_DEV = 1
TOK_DEV = 256


rate_scale = 8.0
norm_eps = 1e-06


def contract(left, right, left_dim, right_dim):
    return lax.dot_general(
        left, right, (((left_dim,), (right_dim,)), ((), ())), preferred_element_type=jnp.float32
    )


def linear_scan(coeffs, values, reverse):

    def combine(earlier, later):
        return (earlier[0] * later[0], later[0] * earlier[1] + later[1])

    return lax.associative_scan(combine, (coeffs, values), axis=0, reverse=reverse)


def silu_grad(values):
    logistic = jax.nn.sigmoid(values)
    return logistic * (1.0 + values * (1.0 - logistic))


def expert_pass(slot_inputs, slot_cotan, gate_local, up_local, down_local):
    gate_pre = contract(slot_inputs, gate_local, 1, 0)
    up_pre = contract(slot_inputs, up_local, 1, 0)
    hidden = (jax.nn.silu(gate_pre) * up_pre).astype(jnp.bfloat16)
    down_wgrad = contract(hidden, slot_cotan, 0, 0)
    hidden_grad = contract(slot_cotan, down_local, 1, 1)
    up_grad = (hidden_grad * jax.nn.silu(gate_pre)).astype(jnp.bfloat16)
    gate_grad = (hidden_grad * up_pre * silu_grad(gate_pre)).astype(jnp.bfloat16)
    gate_wgrad = contract(slot_inputs, gate_grad, 0, 0)
    up_wgrad = contract(slot_inputs, up_grad, 0, 0)
    return (gate_wgrad, up_wgrad, down_wgrad, gate_grad, up_grad)


def block_forward(channels, block_maps):
    shaped = channels.reshape(channels.shape[0], block_maps.shape[0], block_maps.shape[1])
    mapped = jnp.einsum("tkc,kcd->tkd", shaped, block_maps, preferred_element_type=jnp.float32)
    return mapped.reshape(channels.shape)


def block_backward(pre_grad, block_maps):
    shaped = pre_grad.reshape(pre_grad.shape[0], block_maps.shape[0], block_maps.shape[2])
    mapped = jnp.einsum(
        "tkd,kcd->tkc", shaped, block_maps.astype(jnp.float32), precision=lax.Precision.HIGHEST
    )
    return mapped.reshape(pre_grad.shape)


def recurrence_back(adjoint, state_run, conv_float, gate_parts, decay_local, input_local):
    decay_gate, input_gate, decay_base, decay_rate, drive_scale, drive_term = gate_parts
    log_grad = (
        adjoint * (state_run - drive_term)
        - adjoint * input_gate * conv_float * decay_rate * decay_rate / drive_scale
    )
    decay_pre_grad = log_grad * (-rate_scale * decay_base) * decay_gate * (1.0 - decay_gate)
    input_pre_grad = adjoint * drive_scale * conv_float * input_gate * (1.0 - input_gate)
    return (
        adjoint * drive_scale * input_gate
        + block_backward(decay_pre_grad, decay_local)
        + block_backward(input_pre_grad, input_local)
    )


def body(
    out_grad,
    stream,
    norm_gain,
    routes,
    route_weight,
    gate_weight,
    up_weight,
    down_weight,
    out_proj,
    conv_out,
    gate_branch,
    decay_map,
    input_map,
    decay_param,
    decay_shift,
    states,
):
    sources = lax.axis_size("sp")
    quarters = lax.axis_size("tp")
    experts = EXP_DEV * sources
    capacity = (5 * TOP * TOK_DEV + 4 * experts - 1) // (4 * experts)
    token_count, model_width = stream.shape
    stream_f = stream.astype(jnp.float32)
    row_scale = lax.rsqrt(jnp.mean(stream_f * stream_f, axis=1, keepdims=True) + norm_eps)
    unit_rows = stream_f * row_scale
    gain_row = norm_gain.astype(jnp.float32)[None, :]
    normed = (unit_rows * gain_row).astype(jnp.bfloat16)
    pair_expert = routes.reshape(-1)
    pair_count = pair_expert.shape[0]
    onehot = (pair_expert[:, None] == jnp.arange(experts, dtype=jnp.int32)[None, :]).astype(
        jnp.int32
    )
    slot_rank = jnp.sum((jnp.cumsum(onehot, axis=0) - onehot) * onehot, axis=1)
    slot_index = pair_expert * capacity + slot_rank
    slot_pair = (
        jnp.full((experts * capacity,), pair_count, jnp.int32)
        .at[slot_index]
        .set(jnp.arange(pair_count, dtype=jnp.int32))
    )
    slot_token = slot_pair // TOP
    weight_pad = jnp.concatenate([route_weight.reshape(-1), jnp.zeros((1,), jnp.float32)])
    slot_weight = weight_pad[slot_pair][:, None]
    column_width = model_width // quarters
    column_start = lax.axis_index("tp") * column_width
    normed_cols = lax.dynamic_slice_in_dim(normed, column_start, column_width, 1)
    zero_row = jnp.zeros((1, normed_cols.shape[1]), jnp.bfloat16)
    slot_inputs = jnp.concatenate([normed_cols, zero_row])[slot_token]
    slot_cotan = (
        slot_weight
        * jnp.concatenate(
            [lax.dynamic_slice_in_dim(out_grad, column_start, column_width, 1), zero_row]
        )[slot_token].astype(jnp.float32)
    ).astype(jnp.bfloat16)
    part_inputs, part_cotan = (
        lax.all_to_all(slot_inputs, "sp", split_axis=0, concat_axis=0, tiled=True),
        lax.all_to_all(slot_cotan, "sp", split_axis=0, concat_axis=0, tiled=True),
    )
    got_inputs, got_cotan = (
        lax.all_gather(part_inputs, "tp", axis=1, tiled=True),
        lax.all_gather(part_cotan, "tp", axis=1, tiled=True),
    )

    def by_expert(slot_block):
        shaped = slot_block.reshape(sources, EXP_DEV, capacity, model_width)
        return jnp.swapaxes(shaped, 0, 1).reshape(EXP_DEV, sources * capacity, model_width)

    expert_inputs = by_expert(got_inputs)
    expert_cotan = by_expert(got_cotan)
    gate_grads, up_grads, down_grads, partials = ([], [], [], [])
    gate_wgrad, up_wgrad, down_wgrad, gate_grad, up_grad = expert_pass(
        expert_inputs[0], expert_cotan[0], gate_weight[0], up_weight[0], down_weight[0]
    )
    gate_grads.append(gate_wgrad.astype(jnp.bfloat16))
    up_grads.append(up_wgrad.astype(jnp.bfloat16))
    down_grads.append(down_wgrad.astype(jnp.bfloat16))
    partials.append(
        (contract(gate_grad, gate_weight[0], 1, 1) + contract(up_grad, up_weight[0], 1, 1)).astype(
            jnp.bfloat16
        )
    )
    partial_slots = jnp.swapaxes(
        jnp.stack(partials).reshape(EXP_DEV, sources, capacity, model_width), 0, 1
    )
    partial_slots = partial_slots.reshape(sources * EXP_DEV * capacity, model_width)
    summed = (
        lax.psum_scatter(partial_slots, "tp", scatter_dimension=1, tiled=True)
        .astype(jnp.float32)
        .astype(jnp.bfloat16)
    )
    part_back = lax.all_to_all(summed, "sp", split_axis=0, concat_axis=0, tiled=True)
    returned = lax.all_gather(part_back, "tp", axis=1, tiled=True)
    normed_grad = jnp.sum(
        returned[slot_index].reshape(token_count, TOP, model_width).astype(jnp.float32), axis=1
    )
    scaled_grad = gain_row * normed_grad
    stream_grad = out_grad.astype(jnp.float32) + row_scale * (
        scaled_grad - unit_rows * jnp.mean(unit_rows * scaled_grad, axis=1, keepdims=True)
    )
    stream_grad_b = stream_grad.astype(jnp.bfloat16)
    total_state = states[0] + states[1]
    gate_float = gate_branch.astype(jnp.float32)
    gelu_gate, gelu_back = jax.vjp(jax.nn.gelu, gate_float)
    lru_out = (total_state * gelu_gate).astype(jnp.bfloat16)
    out_proj_grad = lax.psum_scatter(
        contract(stream_grad_b, lru_out, 0, 0).astype(jnp.bfloat16),
        "sp",
        scatter_dimension=0,
        tiled=True,
    ).astype(jnp.float32)
    lru_out_grad = contract(stream_grad_b, out_proj, 1, 0)
    gate_branch_grad = gelu_back(lru_out_grad * total_state)[0]
    state_grad = lru_out_grad * gelu_gate
    conv_float = conv_out.astype(jnp.float32)
    ones_row = jnp.ones((1, conv_float.shape[1]), jnp.float32)
    saved, summaries = ([], [])
    for direction in range(2):
        decay_gate = jax.nn.sigmoid(block_forward(conv_out, decay_map[direction]))
        input_gate = jax.nn.sigmoid(block_forward(conv_out, input_map[direction]))
        decay_base = jax.nn.softplus(-decay_param[direction])[None, :]
        log_decay = -rate_scale * decay_gate * decay_base + decay_shift[direction]
        decay_rate = jnp.exp(log_decay)
        drive_scale = jnp.sqrt(-jnp.expm1(2.0 * log_decay))
        drive_term = drive_scale * input_gate * conv_float
        if direction == 0:
            reach_coeff, inner_sum = linear_scan(
                jnp.concatenate([decay_rate[1:], ones_row]), state_grad, True
            )
            summaries.append(decay_rate[:1] * reach_coeff[:1])
            summaries.append(decay_rate[:1] * inner_sum[:1])
        else:
            reach_coeff, inner_sum = linear_scan(
                jnp.concatenate([ones_row, decay_rate[:-1]]), state_grad, False
            )
            summaries.append(decay_rate[-1:] * reach_coeff[-1:])
            summaries.append(decay_rate[-1:] * inner_sum[-1:])
        saved.append(
            (
                (decay_gate, input_gate, decay_base, decay_rate, drive_scale, drive_term),
                reach_coeff,
                inner_sum,
            )
        )
    gathered = (
        lax.all_gather(summaries[0], "sp", axis=0, tiled=True),
        lax.all_gather(summaries[1], "sp", axis=0, tiled=True),
        lax.all_gather(summaries[2], "sp", axis=0, tiled=True),
        lax.all_gather(summaries[3], "sp", axis=0, tiled=True),
    )
    device_index = lax.axis_index("sp")
    zero_row = jnp.zeros_like(ones_row)
    from_right = linear_scan(gathered[0], gathered[1], True)[1]
    from_left = linear_scan(gathered[2], gathered[3], False)[1]
    incoming = (
        lax.dynamic_slice_in_dim(jnp.concatenate([from_right[1:], zero_row]), device_index, 1, 0),
        lax.dynamic_slice_in_dim(jnp.concatenate([zero_row, from_left[:-1]]), device_index, 1, 0),
    )
    conv_grad = jnp.zeros_like(conv_float)
    for direction in range(2):
        gate_parts, reach_coeff, inner_sum = saved[direction]
        adjoint = inner_sum + reach_coeff * incoming[direction]
        conv_grad = conv_grad + recurrence_back(
            adjoint,
            states[direction],
            conv_float,
            gate_parts,
            decay_map[direction],
            input_map[direction],
        )
    return (
        conv_grad,
        gate_branch_grad,
        out_proj_grad,
        jnp.stack(gate_grads),
        jnp.stack(up_grads),
        jnp.stack(down_grads),
    )


def solution(mesh):
    placed = (
        P("sp", None),
        P("sp", None),
        P(),
        P("sp", None),
        P("sp", None),
        P("sp", None, "tp"),
        P("sp", None, "tp"),
        P("sp", "tp", None),
        P(None, "tp"),
        P("sp", "tp"),
        P("sp", "tp"),
        P(None, "tp", None, None),
        P(None, "tp", None, None),
        P(None, "tp"),
        P(None, "sp", "tp"),
        P(None, "sp", "tp"),
    )
    return jax.shard_map(
        body,
        mesh=mesh,
        in_specs=placed,
        out_specs=(
            P("sp", "tp"),
            P("sp", "tp"),
            P("sp", "tp"),
            P("sp", None, "tp"),
            P("sp", None, "tp"),
            P("sp", "tp", None),
        ),
        check_vma=False,
    )
```

profile of v0, /device:TPU:0, one launch (start us, length us, event | category | flops | bytes accessed | tf_op | source)
XLA Modules:
  0.0 486.6 jit_solution(14544216443811962817)
XLA Ops:
  15.6 4.2 convert_multiply_fusion
  21.2 3.5 gather_fusion.2
  24.6 38.8 %all_to_all.33 = bf16[8,80,1024]{2,1,0:T(8,128)(2,1)} all-to-all(bf16[8,80,1024]{2,1,0:T(8,128)(2,1)} %bitcast.189), channel_id=1, replica_groups=mesh['sp'=8,'tp'=4] {'sp'}, dimensions={0} | all-to-all | bytes 2621440 | tf_op jit(solution)/shard_map/all_to_all | solution.py:131
  67.8 3.5 gather_fusion.1
  73.3 34.3 %all_to_all.34 = bf16[8,80,1024]{2,1,0:T(8,128)(2,1)} all-to-all(bf16[8,80,1024]{2,1,0:T(8,128)(2,1)S(1)} %fusion.4), channel_id=1, replica_groups=mesh['sp'=8,'tp'=4] {'sp'}, dimensions={0} | all-to-all | bytes 2621440 | tf_op jit(solution)/shard_map/all_to_all | solution.py:132
  108.0 4.2 fusion.7
  114.3 32.9 %all-gather.8.cloned.1.call-done = bf16[640,4096]{1,0:T(8,128)(2,1)} async-done(((bf16[640,1024]{1,0:T(8,128)(2,1)}), bf16[640,4096]{1,0:T(8,128)(2,1)}) %all-gather.8.cloned.1.call-update) | async-done | bytes 5242896 | tf_op jit(solution)/shard_map/all_gather | solution.py:136
  147.1 4.8 multiply_convert_fusion.1
  153.8 3.8 add_convert_fusion
  157.7 51.3 %reduce-scatter.3.cloned.1.call-done = bf16[640,1024]{1,0:T(8,128)(2,1)} async-done(((bf16[640,4096]{1,0:T(8,128)(2,1)}), bf16[640,1024]{1,0:T(8,128)(2,1)}) %reduce-scatter.3.cloned.1.call-update) | async-done | bytes 1310736 | tf_op jit(solution)/shard_map/reduce_scatter | solution.py:162
  209.0 36.8 %all_to_all.35 = bf16[8,80,1024]{2,1,0:T(8,128)(2,1)} all-to-all(bf16[8,80,1024]{2,1,0:T(8,128)(2,1)} %bitcast.190), channel_id=1, replica_groups=mesh['sp'=8,'tp'=4] {'sp'}, dimensions={0} | all-to-all | bytes 2621440 | tf_op jit(solution)/shard_map/all_to_all | solution.py:166
  251.8 7.3 %fusion.1 = bf16[1,4096,256]{2,1,0:T(8,128)(2,1)} fusion(bf16[640,4096]{1,0:T(8,128)(2,1)} %all-gather.10.cloned.1.call-done, bf16[640,256]{1,0:T(8,128)(2,1)S(1)} %copy-done.15), kind=kOutput, calls=%fused_computation.13 | convolution fusion | flops 1343225856 | bytes 7667712 | tf_op jit(solution)/shard_map/dot_general | solution.py:16
  259.2 3.2 fusion
  262.4 3.3 fusion.2
  265.7 18.8 %all-gather.12.cloned.1.call-done = bf16[640,4096]{1,0:T(8,128)(2,1)} async-done(((bf16[640,1024]{1,0:T(8,128)(2,1)}), bf16[640,4096]{1,0:T(8,128)(2,1)}) %all-gather.12.cloned.1.call-update) | async-done | bytes 5242896 | tf_op jit(solution)/shard_map/all_gather | solution.py:167
  284.5 11.8 %gather_fusion.3 = bf16[512,4096]{1,0:T(8,128)(2,1)} fusion(bf16[640,4096]{1,0:T(8,128)(2,1)} %all-gather.12.cloned.1.call-done, s32[1024]{0:T(1024)S(1)} %pad_clamp_fusion), kind=kCustom, calls=%fused_computation.3 | custom fusion | bytes 8390656 | tf_op jit(solution)/shard_map/gather | solution.py:169
  296.4 9.6 %reshape.201 = f32[256,2,4096]{2,1,0:T(2,128)} reshape(bf16[512,4096]{1,0:T(8,128)(2,1)} %gather_fusion.3) | data formatting | bytes 12582912 | tf_op jit(solution)/shard_map/convert_element_type | solution.py:169
  306.0 13.9 %reduce_sum.41 = f32[256,4096]{1,0:T(8,128)} reduce(f32[256,2,4096]{2,1,0:T(2,128)} %reshape.201, f32[]{:T(128)} %constant.27.clone.1), dimensions={1}, to_apply=%region_6.7 | reduce | flops 1048576 | bytes 12582916 | tf_op jit(solution)/shard_map/reduce_sum | solution.py:168
  329.2 3.7 fusion.35
  338.4 20.5 %all-gather.1 = f32[8,1,256]{2,1,0:T(1,128)S(1)} all-gather(f32[1,1,256]{2,1,0:T(1,128)S(1)} %get-tuple-element.16), channel_id=1, replica_groups=mesh['sp'=8,'tp'=4] {'sp'}, dimensions={0}, use_global_device_ids=true | all-gather | bytes 9216 | tf_op jit(solution)/shard_map/all_gather | solution.py:220
  359.0 16.3 %all-gather = f32[8,1,256]{2,1,0:T(1,128)S(1)} all-gather(f32[1,1,256]{2,1,0:T(1,128)S(1)} %get-tuple-element.17), channel_id=1, replica_groups=mesh['sp'=8,'tp'=4] {'sp'}, dimensions={0}, use_global_device_ids=true | all-gather | bytes 9216 | tf_op jit(solution)/shard_map/all_gather | solution.py:221
  377.0 18.3 %all-gather.3 = f32[8,1,256]{2,1,0:T(1,128)S(1)} all-gather(f32[1,1,256]{2,1,0:T(1,128)S(1)} %get-tuple-element.12), channel_id=1, replica_groups=mesh['sp'=8,'tp'=4] {'sp'}, dimensions={0}, use_global_device_ids=true | all-gather | bytes 9216 | tf_op jit(solution)/shard_map/all_gather | solution.py:222
  395.3 16.3 %all-gather.2 = f32[8,1,256]{2,1,0:T(1,128)S(1)} all-gather(f32[1,1,256]{2,1,0:T(1,128)S(1)} %get-tuple-element.13), channel_id=1, replica_groups=mesh['sp'=8,'tp'=4] {'sp'}, dimensions={0}, use_global_device_ids=true | all-gather | bytes 9216 | tf_op jit(solution)/shard_map/all_gather | solution.py:223
  424.9 53.1 %reduce-scatter.5.cloned.1.call-done = bf16[512,256]{1,0:T(8,128)(2,1)} async-done(((bf16[4096,256]{1,0:T(8,128)(2,1)}), bf16[512,256]{1,0:T(8,128)(2,1)}) %reduce-scatter.5.cloned.1.call-update) | async-done | bytes 262160 | tf_op jit(solution)/shard_map/reduce_scatter | solution.py:180
  (491 shorter events, 56.0 us)
Async XLA Ops:
  7.2 100.8 %copy-start = (bf16[1,4096,256]{2,1,0:T(8,128)(2,1)S(1)}, bf16[1,4096,256]{2,1,0:T(8,128)(2,1)}, u32[]{:S(2)}) copy-start(bf16[1,4096,256]{2,1,0:T(8,128)(2,1)} %param.21) | copy-start | bytes 6291460
  7.2 100.8 %all-gather.10.cloned.1.call-start = ((), (), s32[]{:S(2)}) async-start(), calls=%async_computation.6 | async-start | bytes 6553600 | tf_op jit(solution)/shard_map/all_gather | solution.py:135
  9.2 10.6 %copy-start.27 = (bf16[4096]{0:T(1024)(128)(2,1)S(1)}, bf16[4096]{0:T(1024)(128)(2,1)}, u32[]{:S(2)}) copy-start(bf16[4096]{0:T(1024)(128)(2,1)} %param.18) | copy-start | bytes 24580
  11.3 8.5 %copy-start.28 = (f32[256]{0:T(256)}, f32[256]{0:T(256)S(1)}, u32[]{:S(2)}) copy-start(f32[256]{0:T(256)S(1)} %add_rsqrt_fusion) | copy-start | bytes 3076
  21.2 42.3 %copy-start.39 = (f32[256,2]{0,1:T(2,128)S(1)}, f32[256,2]{0,1:T(2,128)}, u32[]{:S(2)}) copy-start(f32[256,2]{0,1:T(2,128)} %param.20) | copy-start | bytes 6148
  63.5 83.7 %all-gather.8.cloned.1.call-start = ((), (), s32[]{:S(2)}) async-start(), calls=%async_computation.5 | async-start | bytes 6553600 | tf_op jit(solution)/shard_map/all_gather | solution.py:136
  107.6 101.4 %reduce-scatter.3.cloned.1.call-start = ((), (), s32[]{:S(2)}) async-start(), calls=%async_computation.7 | async-start | bytes 6553600 | tf_op jit(solution)/shard_map/reduce_scatter | solution.py:162
  112.7 34.4 %copy-start.47 = (f32[640,256]{1,0:T(8,128)}, f32[640,256]{1,0:T(8,128)S(1)}, u32[]{:S(2)}) copy-start(f32[640,256]{1,0:T(8,128)S(1)} %fusion.7) | copy-start | bytes 1966084
  114.2 37.7 %copy-start.49 = (f32[640,256]{1,0:T(8,128)}, f32[640,256]{1,0:T(8,128)S(1)}, u32[]{:S(2)}) copy-start(f32[640,256]{1,0:T(8,128)S(1)} %fusion.10) | copy-start | bytes 1966084
  157.7 88.8 %copy-start.40 = (f32[2,256]{1,0:T(2,128)S(1)}, f32[2,256]{1,0:T(2,128)}, u32[]{:S(2)}) copy-start(f32[2,256]{1,0:T(2,128)} %param.29) | copy-start | bytes 6148
  157.7 88.9 %copy-start.10 = (bf16[256,256]{1,0:T(8,128)(2,1)S(1)}, bf16[256,256]{1,0:T(8,128)(2,1)}, u32[]{:S(2)}) copy-start(bf16[256,256]{1,0:T(8,128)(2,1)} %param.25) | copy-start | bytes 393220
  157.7 88.9 %copy-start.44 = (bf16[2,1,256,256]{3,2,1,0:T(8,128)(2,1)S(1)}, bf16[2,1,256,256]{3,2,1,0:T(8,128)(2,1)}, u32[]{:S(2)}) copy-start(bf16[2,1,256,256]{3,2,1,0:T(8,128)(2,1)} %param.27) | copy-start | bytes 786436
  157.7 89.1 %copy-start.8 = (f32[2,256,256]{2,1,0:T(8,128)S(1)}, f32[2,256,256]{2,1,0:T(8,128)}, u32[]{:S(2)}) copy-start(f32[2,256,256]{2,1,0:T(8,128)} %param.30) | copy-start | bytes 1572868
  157.7 126.8 %all-gather.12.cloned.1.call-start = ((), (), s32[]{:S(2)}) async-start(), calls=%async_computation.8 | async-start | bytes 6553600 | tf_op jit(solution)/shard_map/all_gather | solution.py:167
  245.9 232.1 %reduce-scatter.5.cloned.1.call-start = ((), (), s32[]{:S(2)}) async-start(), calls=%async_computation.9 | async-start | bytes 2359296 | tf_op jit(solution)/shard_map/reduce_scatter | solution.py:180
  250.9 8.3 %slice-start = ((s8[5242880]{0:T(1024)(128)(4,1)}), s8[4194304]{0:T(1024)(128)(4,1)S(1)}, s32[]{:S(2)}) async-start(s8[5242880]{0:T(1024)(128)(4,1)} %bitcast.218), calls=%async_computation.10 | async-start | bytes 8388608
  251.8 7.3 %slice-start.1 = ((s8[5242880]{0:T(1024)(128)(4,1)}), s8[1048576]{0:T(1024)(128)(4,1)S(1)}, s32[]{:S(2)}) async-start(s8[5242880]{0:T(1024)(128)(4,1)} %bitcast.218), calls=%async_computation.11 | async-start | bytes 2097152
  251.8 10.6 %slice-start.2 = ((s8[5242880]{0:T(1024)(128)(4,1)}), s8[4194304]{0:T(1024)(128)(4,1)S(1)}, s32[]{:S(2)}) async-start(s8[5242880]{0:T(1024)(128)(4,1)} %bitcast.220), calls=%async_computation.12 | async-start | bytes 8388608
  306.0 13.9 %copy-start.3 = (bf16[256,4096]{1,0:T(8,128)(2,1)S(1)}, bf16[256,4096]{1,0:T(8,128)(2,1)}, u32[]{:S(2)}) copy-start(bf16[256,4096]{1,0:T(8,128)(2,1)} %param.17) | copy-start | bytes 6291460
  337.6 39.3 %copy-start.38 = (f32[1,256]{1,0:T(1,128)S(1)}, f32[1,256]{1,0:T(1,128)}, u32[]{:S(2)}) copy-start(f32[1,256]{1,0:T(1,128)} %get-tuple-element.14) | copy-start | bytes 3076
  376.8 41.0 %copy-start.11 = (bf16[256,256]{1,0:T(8,128)(2,1)S(1)}, bf16[256,256]{1,0:T(8,128)(2,1)}, u32[]{:S(2)}) copy-start(bf16[256,256]{1,0:T(8,128)(2,1)} %param.25) | copy-start | bytes 393220
  413.5 8.6 %copy-start.35 = (f32[1,256]{1,0:T(1,128)S(1)}, f32[1,256]{1,0:T(1,128)}, u32[]{:S(2)}) copy-start(f32[1,256]{1,0:T(1,128)} %copy-done.34) | copy-start | bytes 3076
  413.7 8.5 %copy-start.18 = (f32[256,256]{1,0:T(8,128)S(1)}, f32[256,256]{1,0:T(8,128)}, u32[]{:S(2)}) copy-start(f32[256,256]{1,0:T(8,128)} %copy-done.17) | copy-start | bytes 786436
  417.8 62.0 %copy-start.1 = (bf16[1,4096,256]{2,1,0:T(8,128)(2,1)S(1)}, bf16[1,4096,256]{2,1,0:T(8,128)(2,1)}, u32[]{:S(2)}) copy-start(bf16[1,4096,256]{2,1,0:T(8,128)(2,1)} %param.21) | copy-start | bytes 6291460
  (36 other events, 112.3 us)
Sparse Core Ops, SparseCore 0:
  63.6 39.4 all-gather.9
  107.7 39.3 all-gather.7
  157.8 51.1 reduce-scatter.2
  246.0 38.4 all-gather.11
  411.8 66.1 reduce-scatter.4
where the time goes:
time: 492 us; the launch traced here: 487 us
  blocking collectives  181 us (37%)
  waiting for transfers between devices  156 us (32%)
  local copies, waits for them, and re-layouts  49.9 us (10%)
  matrix products  45.7 us (9%)
  other arithmetic  36.2 us (7%)
  between operations  16.3 us (3%)
    reduce_scatter x1, waiting for transfers between devices, body(): lax.psum_scatter(contract(stream_grad_b, lru_out, 0, 0).astype(jnp.bfloat...  53.1 us
    reduce_scatter x1, waiting for transfers between devices, body(): lax.psum_scatter(partial_slots, 'tp', scatter_dimension=1, tiled=True)  51.3 us
    all_to_all x1, blocking collectives, body(): lax.all_to_all(slot_inputs, 'sp', split_axis=0, concat_axis=0, tiled=True)  38.8 us
    all_to_all x1, blocking collectives, body(): lax.all_to_all(summed, 'sp', split_axis=0, concat_axis=0, tiled=True)  36.8 us
    dot_general x10, matrix products, contract(): lax.dot_general(left, right, (((left_dim,), (right_dim,)), ((), ())), pre...  35.6 us
    all_to_all x1, blocking collectives, body(): lax.all_to_all(slot_cotan, 'sp', split_axis=0, concat_axis=0, tiled=True)  34.3 us
    all_gather x1, waiting for transfers between devices, body(): lax.all_gather(part_cotan, 'tp', axis=1, tiled=True)  32.9 us
    all_gather x1, blocking collectives, body(): lax.all_gather(summaries[0], 'sp', axis=0, tiled=True)  20.5 us
  transfers between devices with their start and end apart: 5, of which 4 were waited for; matrix products, arithmetic and copies ran while one was open for 9% of the time, Pallas kernels for 0%

commit v1 on v0

--- a/solution.py
+++ b/solution.py
@@ -164,10 +164,10 @@
         .astype(jnp.bfloat16)
     )
     part_back = lax.all_to_all(summed, "sp", split_axis=0, concat_axis=0, tiled=True)
-    returned = lax.all_gather(part_back, "tp", axis=1, tiled=True)
-    normed_grad = jnp.sum(
-        returned[slot_index].reshape(token_count, TOP, model_width).astype(jnp.float32), axis=1
-    )
+    quarter_grad = jnp.sum(
+        part_back[slot_index].reshape(token_count, TOP, column_width).astype(jnp.float32), axis=1
+    ).astype(jnp.bfloat16)
+    normed_grad = lax.all_gather(quarter_grad, "tp", axis=1, tiled=True).astype(jnp.float32)
     scaled_grad = gain_row * normed_grad
     stream_grad = out_grad.astype(jnp.float32) + row_scale * (
         scaled_grad - unit_rows * jnp.mean(unit_rows * scaled_grad, axis=1, keepdims=True)
@@ -177,12 +177,19 @@
     gate_float = gate_branch.astype(jnp.float32)
     gelu_gate, gelu_back = jax.vjp(jax.nn.gelu, gate_float)
     lru_out = (total_state * gelu_gate).astype(jnp.bfloat16)
-    out_proj_grad = lax.psum_scatter(
-        contract(stream_grad_b, lru_out, 0, 0).astype(jnp.bfloat16),
-        "sp",
-        scatter_dimension=0,
-        tiled=True,
-    ).astype(jnp.float32)
+    lru_rows = lax.all_gather(lru_out, "sp", axis=0, tiled=True)
+    piece_width = column_width // sources
+    own_piece = lax.dynamic_slice_in_dim(
+        stream_grad_b.reshape(token_count, sources, quarters, piece_width),
+        lax.axis_index("tp"),
+        1,
+        2,
+    )[:, :, 0]
+    piece_rows = lax.all_to_all(jnp.swapaxes(own_piece, 0, 1), "sp", split_axis=0, concat_axis=0, tiled=True)
+    grad_rows = lax.all_gather(
+        piece_rows.reshape(sources * token_count, piece_width), "tp", axis=1, tiled=True
+    )
+    out_proj_grad = contract(grad_rows, lru_rows, 0, 0)
     lru_out_grad = contract(stream_grad_b, out_proj, 1, 0)
     gate_branch_grad = gelu_back(lru_out_grad * total_state)[0]
     state_grad = lru_out_grad * gelu_gate
@@ -216,12 +223,7 @@
                 inner_sum,
             )
         )
-    gathered = (
-        lax.all_gather(summaries[0], "sp", axis=0, tiled=True),
-        lax.all_gather(summaries[1], "sp", axis=0, tiled=True),
-        lax.all_gather(summaries[2], "sp", axis=0, tiled=True),
-        lax.all_gather(summaries[3], "sp", axis=0, tiled=True),
-    )
+    gathered = lax.all_gather(jnp.concatenate(summaries, axis=0), "sp", axis=1, tiled=False)
     device_index = lax.axis_index("sp")
     zero_row = jnp.zeros_like(ones_row)
     from_right = linear_scan(gathered[0], gathered[1], True)[1]

time: 492 us -> 413 us (0.84)
  blocking collectives: 181 us -> 104 us
  starting transfers between devices: 1.02 us -> 11.4 us
  other arithmetic: 36.2 us -> 29.4 us
    reduce_scatter x1 -> x0, waiting for transfers between devices: 53.1 us -> none  [body(): lax.psum_scatter(contract(stream_grad_b, lru_out, 0, 0).astype(jnp.bfloat...]
    all_gather x4 -> x1, blocking collectives: 71.4 us -> 30.7 us  [body(): lax.all_gather(jnp.concatenate(summaries, axis=0), 'sp', axis=1, tiled=Fa...]
    all_to_all x1 -> x0, blocking collectives: 36.8 us -> none  [body(): lax.all_to_all(summed, 'sp', split_axis=0, concat_axis=0, tiled=True)]
    all_to_all x0 -> x2, waiting for transfers between devices: none -> 32.5 us  [the longest x1 31.2 us: body(): lax.all_to_all(summed, 'sp', split_axis=0, concat_axis=0, tiled=True)]
    all_gather x1 -> x3, waiting for transfers between devices: 18.8 us -> 38.6 us  [the longest x1 23.5 us: body(): lax.all_gather(piece_rows.reshape(sources * token_count, piece_width), 't...]
    all_to_all x0 -> x2, starting transfers between devices: none -> 11 us  [the longest x1 5.52 us: body(): lax.all_to_all(summed, 'sp', split_axis=0, concat_axis=0, tiled=True)]
    reduce_sum x1, other arithmetic: 13.9 us -> 3.59 us  [body(): jnp.sum(part_back[slot_index].reshape(token_count, TOP, column_width).ast...]
    gather x1, local copies, waits for them, and re-layouts: 11.8 us -> 2.05 us  [body(): part_back[slot_index].reshape(token_count, TOP, column_width)]
  transfers between devices with their start and end apart: 5 -> 8, of which waited for: 4 -> 7; matrix products, arithmetic and copies ran while one was open for 9% -> 13% of each run, Pallas kernels for 0% -> 0%
where the time goes in v1:
time: 413 us; the launch traced here: 408 us
  waiting for transfers between devices  155 us (38%)
  blocking collectives  104 us (25%)
  local copies, waits for them, and re-layouts  47.5 us (12%)
  matrix products  43.8 us (11%)
  other arithmetic  29.4 us (7%)
  between operations  17 us (4%)
  starting transfers between devices  11.4 us (3%)
    reduce_scatter x1, waiting for transfers between devices, body(): lax.psum_scatter(partial_slots, 'tp', scatter_dimension=1, tiled=True)  51.3 us
    all_to_all x1, blocking collectives, body(): lax.all_to_all(slot_inputs, 'sp', split_axis=0, concat_axis=0, tiled=True)  38.9 us
    dot_general x10, matrix products, contract(): lax.dot_general(left, right, (((left_dim,), (right_dim,)), ((), ())), pre...  36.4 us
    all_to_all x1, blocking collectives, body(): lax.all_to_all(slot_cotan, 'sp', split_axis=0, concat_axis=0, tiled=True)  34.3 us
    all_gather x1, waiting for transfers between devices, body(): lax.all_gather(part_cotan, 'tp', axis=1, tiled=True)  32.2 us
    all_to_all x1, waiting for transfers between devices, body(): lax.all_to_all(summed, 'sp', split_axis=0, concat_axis=0, tiled=True)  31.2 us
    all_gather x1, blocking collectives, body(): lax.all_gather(jnp.concatenate(summaries, axis=0), 'sp', axis=1, tiled=Fa...  30.7 us
    all_gather x1, waiting for transfers between devices, body(): lax.all_gather(piece_rows.reshape(sources * token_count, piece_width), 't...  23.5 us
  transfers between devices with their start and end apart: 8, of which 7 were waited for; matrix products, arithmetic and copies ran while one was open for 13% of the time, Pallas kernels for 0%

profile of v1, /device:TPU:0, one launch (start us, length us, event | category | flops | bytes accessed | tf_op | source)
XLA Modules:
  0.0 407.7 jit_solution(18349608381157708019)
XLA Ops:
  15.6 4.2 %convert_multiply_fusion = f32[256,4096]{1,0:T(8,128)} fusion(bf16[256,4096]{1,0:T(8,128)(2,1)} %param.17, f32[256]{0:T(256)S(1)} %add_rsqrt_fusion), kind=kLoop, calls=%fused_computation.6 | loop fusion | flops 2097152 | bytes 6292480 | tf_op jit(solution)/shard_map/mul | solution.py:101
  21.1 3.5 gather_fusion.2
  24.6 38.9 %all_to_all.38 = bf16[8,80,1024]{2,1,0:T(8,128)(2,1)} all-to-all(bf16[8,80,1024]{2,1,0:T(8,128)(2,1)} %bitcast.179), channel_id=1, replica_groups=mesh['sp'=8,'tp'=4] {'sp'}, dimensions={0} | all-to-all | bytes 2621440 | tf_op jit(solution)/shard_map/all_to_all | solution.py:131
  67.9 3.5 gather_fusion.1
  73.4 34.3 %all_to_all.39 = bf16[8,80,1024]{2,1,0:T(8,128)(2,1)} all-to-all(bf16[8,80,1024]{2,1,0:T(8,128)(2,1)S(1)} %fusion.4), channel_id=1, replica_groups=mesh['sp'=8,'tp'=4] {'sp'}, dimensions={0} | all-to-all | bytes 2621440 | tf_op jit(solution)/shard_map/all_to_all | solution.py:132
  108.0 4.2 %fusion.7 = f32[640,256]{1,0:T(8,128)S(1)} fusion(bf16[640,4096]{1,0:T(8,128)(2,1)} %all-gather.9.cloned.1.call-done, bf16[1,4096,256]{2,1,0:T(8,128)(2,1)S(1)} %copy-done), kind=kOutput, calls=%fused_computation.22 | convolution fusion | flops 1342177280 | bytes 7995392 | tf_op jit(solution)/shard_map/dot_general | solution.py:16
  115.0 32.2 %all-gather.7.cloned.1.call-done = bf16[640,4096]{1,0:T(8,128)(2,1)} async-done(((bf16[640,1024]{1,0:T(8,128)(2,1)}), bf16[640,4096]{1,0:T(8,128)(2,1)}) %all-gather.7.cloned.1.call-update) | async-done | bytes 5242896 | tf_op jit(solution)/shard_map/all_gather | solution.py:136
  147.2 4.9 %multiply_convert_fusion.1 = (bf16[640,256]{1,0:T(8,128)(2,1)S(1)}, bf16[640,256]{1,0:T(8,128)(2,1)S(1)}) fusion(f32[640,256]{1,0:T(8,128)S(1)} %fusion.7, f32[640,256]{1,0:T(8,128)} %fusion.10, bf16[640,4096]{1,0:T(8,128)(2,1)} %all-gather.7.cloned.1.call-done, bf16[1,256,4096]{2,1,0:T(8,128)(2,1)} %param.23), kind=kOutput, calls=%fused_computation.57 | convolution fusion | flops 1344307200 | bytes 9306112 | tf_op jit(solution)/shard_map/dot_general | solution.py:16
  153.9 3.8 add_convert_fusion
  157.8 51.3 %reduce-scatter.2.cloned.1.call-done = bf16[640,1024]{1,0:T(8,128)(2,1)} async-done(((bf16[640,4096]{1,0:T(8,128)(2,1)}), bf16[640,1024]{1,0:T(8,128)(2,1)}) %reduce-scatter.2.cloned.1.call-update) | async-done | bytes 1310736 | tf_op jit(solution)/shard_map/reduce_scatter | solution.py:162
  209.1 5.5 %all-to-all-start.2 = ((bf16[8,80,1024]{2,1,0:T(8,128)(2,1)}), bf16[8,80,1024]{2,1,0:T(8,128)(2,1)S(1)}, u32[]{:S(2)}, u32[]{:S(2)}) async-start(bf16[8,80,1024]{2,1,0:T(8,128)(2,1)} %bitcast.181), calls=%async_computation.3 | async-start | bytes 2621440 | tf_op jit(solution)/shard_map/all_to_all | solution.py:166
  214.7 31.2 %all-to-all-done.2 = bf16[8,80,1024]{2,1,0:T(8,128)(2,1)S(1)} async-done(((bf16[8,80,1024]{2,1,0:T(8,128)(2,1)}), bf16[8,80,1024]{2,1,0:T(8,128)(2,1)S(1)}, u32[]{:S(2)}, u32[]{:S(2)}) %all-to-all-start.2) | async-done | bytes 1310752 | tf_op jit(solution)/shard_map/all_to_all | solution.py:166
  248.4 3.6 reduce_sum.44
  257.5 6.5 %fusion.1 = bf16[1,4096,256]{2,1,0:T(8,128)(2,1)} fusion(bf16[640,4096]{1,0:T(8,128)(2,1)} %all-gather.9.cloned.1.call-done, bf16[640,256]{1,0:T(8,128)(2,1)S(1)} %copy-done.30), kind=kOutput, calls=%fused_computation.12 | convolution fusion | flops 1343225856 | bytes 7667712 | tf_op jit(solution)/shard_map/dot_general | solution.py:16
  264.1 3.2 fusion
  267.3 3.3 fusion.2
  275.7 3.0 add_convert_fusion.1
  278.8 4.6 %reshape.209 = bf16[256,8,4,128]{3,2,1,0:T(4,128)(2,1)} reshape(bf16[256,4096]{1,0:T(8,128)(2,1)} %add_convert_fusion.1) | data formatting | bytes 4194304 | tf_op jit(solution)/shard_map/reshape | solution.py:183
  283.4 3.1 multiply_convert_fusion.4
  300.5 30.7 %all-gather = f32[4,2048]{1,0:T(4,128)S(1)} all-gather(f32[4,256]{1,0:T(4,128)S(1)} %pad_maximum_fusion.23), channel_id=2, replica_groups=mesh['sp'=8,'tp'=4] {'sp'}, dimensions={1}, use_global_device_ids=true | all-gather | bytes 36864 | tf_op jit(solution)/shard_map/all_gather | solution.py:226
  334.1 5.4 %all-to-all-start.3 = ((bf16[8,256,128]{2,1,0:T(8,128)(2,1)}), bf16[8,256,128]{2,1,0:T(8,128)(2,1)S(1)}, u32[]{:S(2)}, u32[]{:S(2)}) async-start(bf16[8,256,128]{2,1,0:T(8,128)(2,1)} %bitcast.171), calls=%async_computation.4 | async-start | bytes 1048576 | tf_op jit(solution)/shard_map/all_to_all | solution.py:188
  360.7 12.8 %all-gather.15.cloned.1.call-done = bf16[2048,256]{1,0:T(8,128)(2,1)} async-done(((bf16[256,256]{1,0:T(8,128)(2,1)}), bf16[2048,256]{1,0:T(8,128)(2,1)}) %all-gather.15.cloned.1.call-update) | async-done | bytes 1048592 | tf_op jit(solution)/shard_map/all_gather | solution.py:180
  373.5 23.5 %all-gather.13.cloned.1.call-done = bf16[2048,512]{1,0:T(8,128)(2,1)} async-done(((bf16[2048,128]{1,0:T(8,128)(2,1)}), bf16[2048,512]{1,0:T(8,128)(2,1)}) %all-gather.13.cloned.1.call-update) | async-done | bytes 2097168 | tf_op jit(solution)/shard_map/all_gather | solution.py:189
  397.0 3.4 fusion.181
  (514 shorter events, 70.1 us)
Async XLA Ops:
  7.2 100.8 %copy-start = (bf16[1,4096,256]{2,1,0:T(8,128)(2,1)S(1)}, bf16[1,4096,256]{2,1,0:T(8,128)(2,1)}, u32[]{:S(2)}) copy-start(bf16[1,4096,256]{2,1,0:T(8,128)(2,1)} %param.21) | copy-start | bytes 6291460
  7.2 100.8 %all-gather.9.cloned.1.call-start = ((), (), s32[]{:S(2)}) async-start(), calls=%async_computation.6 | async-start | bytes 6553600 | tf_op jit(solution)/shard_map/all_gather | solution.py:135
  24.6 39.0 %copy-start.49 = (f32[256,2]{0,1:T(2,128)S(1)}, f32[256,2]{0,1:T(2,128)}, u32[]{:S(2)}) copy-start(f32[256,2]{0,1:T(2,128)} %param.20) | copy-start | bytes 6148
  63.5 83.7 %all-gather.7.cloned.1.call-start = ((), (), s32[]{:S(2)}) async-start(), calls=%async_computation.5 | async-start | bytes 6553600 | tf_op jit(solution)/shard_map/all_gather | solution.py:136
  107.7 101.4 %reduce-scatter.2.cloned.1.call-start = ((), (), s32[]{:S(2)}) async-start(), calls=%async_computation.7 | async-start | bytes 6553600 | tf_op jit(solution)/shard_map/reduce_scatter | solution.py:162
  112.7 34.6 %copy-start.56 = (f32[640,256]{1,0:T(8,128)}, f32[640,256]{1,0:T(8,128)S(1)}, u32[]{:S(2)}) copy-start(f32[640,256]{1,0:T(8,128)S(1)} %fusion.7) | copy-start | bytes 1966084
  209.1 36.7 %all-to-all-start.2 = ((bf16[8,80,1024]{2,1,0:T(8,128)(2,1)}), bf16[8,80,1024]{2,1,0:T(8,128)(2,1)S(1)}, u32[]{:S(2)}, u32[]{:S(2)}) async-start(bf16[8,80,1024]{2,1,0:T(8,128)(2,1)} %bitcast.181), calls=%async_computation.3 | async-start | bytes 2621440 | tf_op jit(solution)/shard_map/all_to_all | solution.py:166
  214.7 58.2 %all-gather.11.cloned.1.call-start = ((), (), s32[]{:S(2)}) async-start(), calls=%async_computation.8 | async-start | bytes 2621440 | tf_op jit(solution)/shard_map/all_gather | solution.py:170
  252.0 121.5 %all-gather.15.cloned.1.call-start = ((), (), s32[]{:S(2)}) async-start(), calls=%async_computation.10 | async-start | bytes 1179648 | tf_op jit(solution)/shard_map/all_gather | solution.py:180
  257.5 9.8 %slice-start.2 = ((s8[5242880]{0:T(1024)(128)(4,1)}), s8[4194304]{0:T(1024)(128)(4,1)S(1)}, s32[]{:S(2)}) async-start(s8[5242880]{0:T(1024)(128)(4,1)} %bitcast.201), calls=%async_computation.13 | async-start | bytes 8388608
  294.5 37.3 %copy-start.5 = (bf16[256,8,4,128]{3,2,1,0:T(4,128)(2,1)S(1)}, bf16[256,8,4,128]{3,2,1,0:T(4,128)(2,1)}, u32[]{:S(2)}) copy-start(bf16[256,8,4,128]{3,2,1,0:T(4,128)(2,1)} %reshape.209) | copy-start | bytes 6291460
  297.0 34.4 %copy-start.19 = (f32[256,256]{1,0:T(8,128)}, f32[256,256]{1,0:T(8,128)S(1)}, u32[]{:S(2)}) copy-start(f32[256,256]{1,0:T(8,128)S(1)} %pad.304) | copy-start | bytes 786436
  297.1 34.3 %copy-start.12 = (f32[256,256]{1,0:T(8,128)}, f32[256,256]{1,0:T(8,128)S(1)}, u32[]{:S(2)}) copy-start(f32[256,256]{1,0:T(8,128)S(1)} %pad.256) | copy-start | bytes 786436
  298.1 33.3 %copy-start.14 = (f32[256,256]{1,0:T(8,128)}, f32[256,256]{1,0:T(8,128)S(1)}, u32[]{:S(2)}) copy-start(f32[256,256]{1,0:T(8,128)S(1)} %pad.272) | copy-start | bytes 786436
  334.1 19.0 %all-to-all-start.3 = ((bf16[8,256,128]{2,1,0:T(8,128)(2,1)}), bf16[8,256,128]{2,1,0:T(8,128)(2,1)S(1)}, u32[]{:S(2)}, u32[]{:S(2)}) async-start(bf16[8,256,128]{2,1,0:T(8,128)(2,1)} %bitcast.171), calls=%async_computation.4 | async-start | bytes 1048576 | tf_op jit(solution)/shard_map/all_to_all | solution.py:188
  339.5 16.4 %copy-start.17 = (f32[256,256]{1,0:T(8,128)S(1)}, f32[256,256]{1,0:T(8,128)}, u32[]{:S(2)}) copy-start(f32[256,256]{1,0:T(8,128)} %pad.305) | copy-start | bytes 786436
  339.5 16.4 %copy-start.18 = (f32[256,256]{1,0:T(8,128)S(1)}, f32[256,256]{1,0:T(8,128)}, u32[]{:S(2)}) copy-start(f32[256,256]{1,0:T(8,128)} %pad.289) | copy-start | bytes 786436
  339.5 16.4 %copy-start.20 = (f32[256,256]{1,0:T(8,128)S(1)}, f32[256,256]{1,0:T(8,128)}, u32[]{:S(2)}) copy-start(f32[256,256]{1,0:T(8,128)} %copy-done.19) | copy-start | bytes 786436
  339.5 16.4 %copy-start.21 = (f32[256,256]{1,0:T(8,128)S(1)}, f32[256,256]{1,0:T(8,128)}, u32[]{:S(2)}) copy-start(f32[256,256]{1,0:T(8,128)} %pad.288) | copy-start | bytes 786436
  339.6 57.5 %all-gather.13.cloned.1.call-start = ((), (), s32[]{:S(2)}) async-start(), calls=%async_computation.9 | async-start | bytes 2621440 | tf_op jit(solution)/shard_map/all_gather | solution.py:189
  341.3 14.7 %copy-start.23 = (f32[2,256,256]{2,1,0:T(8,128)S(1)}, f32[2,256,256]{2,1,0:T(8,128)}, u32[]{:S(2)}) copy-start(f32[2,256,256]{2,1,0:T(8,128)} %param.30) | copy-start | bytes 1572868
  341.3 14.7 %copy-start.26 = (bf16[256,256]{1,0:T(8,128)(2,1)S(1)}, bf16[256,256]{1,0:T(8,128)(2,1)}, u32[]{:S(2)}) copy-start(bf16[256,256]{1,0:T(8,128)(2,1)} %param.25) | copy-start | bytes 393220
  341.4 14.7 %copy-start.38 = (f32[256,256]{1,0:T(8,128)S(1)}, f32[256,256]{1,0:T(8,128)}, u32[]{:S(2)}) copy-start(f32[256,256]{1,0:T(8,128)} %get-tuple-element.109) | copy-start | bytes 786436
  359.5 40.9 %copy-start.1 = (bf16[1,4096,256]{2,1,0:T(8,128)(2,1)S(1)}, bf16[1,4096,256]{2,1,0:T(8,128)(2,1)}, u32[]{:S(2)}) copy-start(bf16[1,4096,256]{2,1,0:T(8,128)(2,1)} %param.21) | copy-start | bytes 6291460
  (47 other events, 163.6 us)
Sparse Core Ops, SparseCore 0:
  63.7 39.4 all-gather.8
  107.8 39.3 all-gather.6
  157.9 51.1 reduce-scatter.1
  252.2 20.6 all-gather.10
  331.5 41.9 all-gather.14
  375.5 21.5 all-gather.12

commit v2 on v1

--- a/solution.py
+++ b/solution.py
@@ -1,6 +1,10 @@
+import functools
+
 import jax
 import jax.numpy as jnp
 from jax import lax
+from jax.experimental import pallas as pl
+from jax.experimental.pallas import tpu as pltpu
 from jax.sharding import PartitionSpec as P
 
 TOP = 2
@@ -71,6 +75,304 @@
         + block_backward(decay_pre_grad, decay_local)
         + block_backward(input_pre_grad, input_local)
     )
+
+
+MESH = pl.DeviceIdType.MESH
+
+
+def push(source, target, send_sem, recv_sem, where):
+    return pltpu.make_async_remote_copy(
+        src_ref=source,
+        dst_ref=target,
+        send_sem=send_sem,
+        recv_sem=recv_sem,
+        device_id=where,
+        device_id_type=MESH,
+    )
+
+
+def greet(sources, me, others):
+    barrier = pltpu.get_barrier_semaphore()
+
+    def one(step, carry):
+        pl.semaphore_signal(
+            barrier, inc=1, device_id={"sp": lax.rem(me + step, sources)}, device_id_type=MESH
+        )
+        return carry
+
+    lax.fori_loop(1, sources, one, 0)
+    for other in others:
+        pl.semaphore_signal(barrier, inc=1, device_id={"tp": other}, device_id_type=MESH)
+    pl.semaphore_wait(barrier, sources - 1 + len(others))
+
+
+def loop(low, high, step):
+    def one(index, carry):
+        step(index)
+        return carry
+
+    lax.fori_loop(low, high, one, 0)
+
+
+def quarter_at(ref, slot, quarter, width):
+    return ref.at[slot, :, pl.ds(pl.multiple_of(quarter * width, width), width)]
+
+
+def dispatch_kernel(
+    sources, in_ref, ct_ref, oin_ref, oct_ref,
+    send_a, recv_a, send_b, recv_b, send_c, recv_c, send_d, recv_d, local
+):
+    me, mine = lax.axis_index("sp"), lax.axis_index("tp")
+    beside = mine + 1 - 2 * lax.rem(mine, 2)
+    across = lax.rem(mine + 2, 4)
+    diagonal = lax.rem(beside + 2, 4)
+    width = in_ref.shape[2]
+    pairs = ((in_ref, oin_ref), (ct_ref, oct_ref))
+    owned = [
+        pltpu.make_async_copy(src.at[me], quarter_at(dst, me, mine, width), local.at[arr])
+        for arr, (src, dst) in enumerate(pairs)
+    ]
+    for copy in owned:
+        copy.start()
+    greet(sources, me, (beside, across))
+
+    def first(arr, peer):
+        src, dst = pairs[arr]
+        return push(
+            src.at[peer], quarter_at(dst, me, mine, width),
+            send_a.at[arr, peer], recv_a.at[arr, me], {"sp": peer},
+        )
+
+    def first_landed(arr, origin):
+        src, dst = pairs[arr]
+        return push(
+            src.at[me], quarter_at(dst, origin, mine, width),
+            send_a.at[arr, me], recv_a.at[arr, origin], {"sp": origin},
+        )
+
+    def passed(arr, slot, quarter, send, recv, target):
+        view = quarter_at(pairs[arr][1], slot, quarter, width)
+        return push(view, view, send.at[arr, slot], recv.at[arr, slot], {"tp": target})
+
+    def start_first(step):
+        peer = lax.rem(me + step, sources)
+        first(0, peer).start()
+        first(1, peer).start()
+
+    loop(1, sources, start_first)
+    for copy in owned:
+        copy.wait()
+
+    def relay(slot):
+        for arr in range(2):
+            passed(arr, slot, mine, send_c, recv_c, across).start()
+            passed(arr, slot, mine, send_b, recv_b, beside).start()
+
+    relay(me)
+
+    def onward(step):
+        slot = lax.rem(me + sources - step, sources)
+        for arr in range(2):
+            passed(arr, slot, across, send_c, recv_c, across).wait_recv()
+            passed(arr, slot, across, send_d, recv_d, beside).start()
+
+    lag = 2
+
+    def steps(step):
+        @pl.when(step < sources)
+        def _():
+            slot = lax.rem(me + sources - step, sources)
+            for arr in range(2):
+                first_landed(arr, slot).wait_recv()
+            relay(slot)
+
+        @pl.when(step >= lag)
+        def _():
+            onward(step - lag)
+
+    loop(1, sources + lag, steps)
+
+    def finish(slot):
+        for arr in range(2):
+            passed(arr, slot, beside, send_b, recv_b, beside).wait_recv()
+            passed(arr, slot, diagonal, send_d, recv_d, beside).wait_recv()
+            passed(arr, slot, mine, send_b, recv_b, beside).wait_send()
+            passed(arr, slot, mine, send_c, recv_c, across).wait_send()
+            passed(arr, slot, across, send_d, recv_d, beside).wait_send()
+
+    loop(0, sources, finish)
+
+    def finish_first(step):
+        peer = lax.rem(me + step, sources)
+        for arr in range(2):
+            first(arr, peer).wait_send()
+
+    loop(1, sources, finish_first)
+
+
+def dispatch(sources, slot_inputs, slot_cotan):
+    _, capacity, width = slot_inputs.shape
+    rows = jax.ShapeDtypeStruct((sources, capacity, 4 * width), slot_inputs.dtype)
+    two = pltpu.SemaphoreType.DMA((2, sources))
+    return pl.pallas_call(
+        functools.partial(dispatch_kernel, sources),
+        out_shape=(rows, rows),
+        in_specs=[pl.BlockSpec(memory_space=pltpu.VMEM)] * 2,
+        out_specs=[pl.BlockSpec(memory_space=pl.ANY)] * 2,
+        scratch_shapes=[two] * 8 + [pltpu.SemaphoreType.DMA((2,))],
+        compiler_params=pltpu.CompilerParams(collective_id=0, has_side_effects=True),
+    )(slot_inputs, slot_cotan)
+
+
+def return_kernel(
+    sources, part_ref, lru_ref, out_ref, olru_ref, near, paired, distant, total,
+    send_a, recv_a, send_b, recv_b, send_c, recv_c, send_l, recv_l, local
+):
+    me, mine = lax.axis_index("sp"), lax.axis_index("tp")
+    beside = mine + 1 - 2 * lax.rem(mine, 2)
+    across = lax.rem(mine + 2, 4)
+    diagonal = lax.rem(beside + 2, 4)
+    width = total.shape[2]
+    greet(sources, me, (beside, across))
+
+    def load(slot, quarter):
+        columns = pl.ds(pl.multiple_of(quarter * width, width), width)
+        return part_ref[slot, :, columns].astype(jnp.float32)
+
+    def near_copy(slot, place, quarter):
+        return push(
+            quarter_at(part_ref, slot, quarter, width), near.at[slot, place],
+            send_a.at[slot, place], recv_a.at[slot, place], {"tp": beside},
+        )
+
+    def far_copy(slot):
+        return push(
+            paired.at[slot], distant.at[slot], send_b.at[slot], recv_b.at[slot], {"tp": across}
+        )
+
+    def home_copy(peer, slot):
+        return push(
+            total.at[peer], out_ref.at[slot], send_c.at[peer], recv_c.at[slot], {"sp": peer}
+        )
+
+    def own_copy():
+        return pltpu.make_async_copy(total.at[me], out_ref.at[me], local.at[0])
+
+    def lru_copy(peer, slot):
+        return push(lru_ref, olru_ref.at[slot], send_l.at[peer], recv_l.at[slot], {"sp": peer})
+
+    def start_lru(step):
+        peer = lax.rem(me + step, sources)
+        lru_copy(peer, me).start()
+
+    lru_own = pltpu.make_async_copy(lru_ref, olru_ref.at[me], local.at[1])
+    lru_own.start()
+    def begin(step):
+        slot = lax.rem(me + 1 + step, sources)
+        near_copy(slot, 1, diagonal).start()
+        near_copy(slot, 0, beside).start()
+
+    loop(0, sources, begin)
+    loop(1, sources, start_lru)
+    lag = 2
+
+    def steps(step):
+        @pl.when(step < sources)
+        def _():
+            slot = lax.rem(me + 1 + step, sources)
+            near_copy(slot, 1, diagonal).wait_recv()
+            paired[slot] = (load(slot, across) + near[slot, 1].astype(jnp.float32)).astype(
+                jnp.bfloat16
+            )
+            far_copy(slot).start()
+
+        @pl.when(step >= lag)
+        def _():
+            slot = lax.rem(me + 1 + step - lag, sources)
+            near_copy(slot, 0, beside).wait_recv()
+            far_copy(slot).wait_recv()
+            total[slot] = (
+                load(slot, mine)
+                + near[slot, 0].astype(jnp.float32)
+                + distant[slot].astype(jnp.float32)
+            ).astype(jnp.bfloat16)
+
+            @pl.when(step < sources + lag - 1)
+            def _():
+                home_copy(slot, me).start()
+
+    loop(0, sources + lag, steps)
+    own_copy().start()
+
+    def finish(step):
+        peer = lax.rem(me + step, sources)
+        home_copy(peer, peer).wait_recv()
+        home_copy(peer, me).wait_send()
+        lru_copy(peer, me).wait_send()
+        lru_copy(peer, peer).wait_recv()
+
+    loop(1, sources, finish)
+
+    def finish_tp(slot):
+        near_copy(slot, 0, beside).wait_send()
+        near_copy(slot, 1, diagonal).wait_send()
+        far_copy(slot).wait_send()
+
+    loop(0, sources, finish_tp)
+    own_copy().wait()
+    lru_own.wait()
+
+
+def return_rows(sources, partial, lru_out):
+    _, capacity, model_width = partial.shape
+    width = model_width // 4
+    held = pltpu.VMEM((sources, capacity, width), jnp.bfloat16)
+    two = pltpu.SemaphoreType.DMA((sources, 2))
+    one = pltpu.SemaphoreType.DMA((sources,))
+    return pl.pallas_call(
+        functools.partial(return_kernel, sources),
+        out_shape=(
+            jax.ShapeDtypeStruct((sources, capacity, width), jnp.bfloat16),
+            jax.ShapeDtypeStruct((sources,) + lru_out.shape, lru_out.dtype),
+        ),
+        in_specs=[pl.BlockSpec(memory_space=pltpu.VMEM)] * 2,
+        out_specs=[pl.BlockSpec(memory_space=pl.ANY)] * 2,
+        scratch_shapes=[
+            pltpu.VMEM((sources, 2, capacity, width), jnp.bfloat16), held, held, held,
+            two, two, one, one, one, one, one, one, pltpu.SemaphoreType.DMA((2,)),
+        ],
+        compiler_params=pltpu.CompilerParams(collective_id=1, has_side_effects=True),
+    )(partial, lru_out)
+
+
+def share_kernel(sources, own_ref, out_ref, send_a, recv_a):
+    me = lax.axis_index("sp")
+    greet(sources, me, ())
+    out_ref[me] = own_ref[...]
+
+    def copy(peer, slot):
+        return push(own_ref, out_ref.at[slot], send_a.at[peer], recv_a.at[slot], {"sp": peer})
+
+    loop(1, sources, lambda step: copy(lax.rem(me + step, sources), me).start())
+
+    def finish(step):
+        peer = lax.rem(me + step, sources)
+        copy(peer, peer).wait_recv()
+        copy(peer, me).wait_send()
+
+    loop(1, sources, finish)
+
+
+def share(sources, own):
+    one = pltpu.SemaphoreType.DMA((sources,))
+    return pl.pallas_call(
+        functools.partial(share_kernel, sources),
+        out_shape=jax.ShapeDtypeStruct((sources,) + own.shape, own.dtype),
+        in_specs=[pl.BlockSpec(memory_space=pltpu.VMEM)],
+        out_specs=pl.BlockSpec(memory_space=pltpu.VMEM),
+        scratch_shapes=[one, one],
+        compiler_params=pltpu.CompilerParams(collective_id=2, has_side_effects=True),
+    )(own)
 
 
 def body(
@@ -108,40 +410,28 @@
     )
     slot_rank = jnp.sum((jnp.cumsum(onehot, axis=0) - onehot) * onehot, axis=1)
     slot_index = pair_expert * capacity + slot_rank
-    slot_pair = (
-        jnp.full((experts * capacity,), pair_count, jnp.int32)
-        .at[slot_index]
-        .set(jnp.arange(pair_count, dtype=jnp.int32))
-    )
-    slot_token = slot_pair // TOP
-    weight_pad = jnp.concatenate([route_weight.reshape(-1), jnp.zeros((1,), jnp.float32)])
-    slot_weight = weight_pad[slot_pair][:, None]
+    places = slot_index.reshape(token_count, TOP, 1) == jnp.arange(
+        experts * capacity, dtype=jnp.int32
+    )
+    chosen = jnp.any(places, axis=1).astype(jnp.bfloat16)
+    slot_weight = jnp.sum(jnp.where(places, route_weight[:, :, None], 0.0), axis=(0, 1))[:, None]
     column_width = model_width // quarters
     column_start = lax.axis_index("tp") * column_width
     normed_cols = lax.dynamic_slice_in_dim(normed, column_start, column_width, 1)
-    zero_row = jnp.zeros((1, normed_cols.shape[1]), jnp.bfloat16)
-    slot_inputs = jnp.concatenate([normed_cols, zero_row])[slot_token]
-    slot_cotan = (
-        slot_weight
-        * jnp.concatenate(
-            [lax.dynamic_slice_in_dim(out_grad, column_start, column_width, 1), zero_row]
-        )[slot_token].astype(jnp.float32)
-    ).astype(jnp.bfloat16)
-    part_inputs, part_cotan = (
-        lax.all_to_all(slot_inputs, "sp", split_axis=0, concat_axis=0, tiled=True),
-        lax.all_to_all(slot_cotan, "sp", split_axis=0, concat_axis=0, tiled=True),
-    )
-    got_inputs, got_cotan = (
-        lax.all_gather(part_inputs, "tp", axis=1, tiled=True),
-        lax.all_gather(part_cotan, "tp", axis=1, tiled=True),
-    )
-
-    def by_expert(slot_block):
-        shaped = slot_block.reshape(sources, EXP_DEV, capacity, model_width)
-        return jnp.swapaxes(shaped, 0, 1).reshape(EXP_DEV, sources * capacity, model_width)
-
-    expert_inputs = by_expert(got_inputs)
-    expert_cotan = by_expert(got_cotan)
+    grad_cols = lax.dynamic_slice_in_dim(out_grad, column_start, column_width, 1)
+    slot_inputs = contract(chosen, normed_cols, 0, 0).astype(jnp.bfloat16)
+    slot_cotan = (slot_weight * contract(chosen, grad_cols, 0, 0)).astype(jnp.bfloat16)
+    total_state = states[0] + states[1]
+    gate_float = gate_branch.astype(jnp.float32)
+    gelu_gate, gelu_back = jax.vjp(jax.nn.gelu, gate_float)
+    lru_out = (total_state * gelu_gate).astype(jnp.bfloat16)
+    got_inputs, got_cotan = dispatch(
+        sources,
+        slot_inputs.reshape(sources, capacity, column_width),
+        slot_cotan.reshape(sources, capacity, column_width),
+    )
+    expert_inputs = got_inputs.reshape(1, sources * capacity, model_width)
+    expert_cotan = got_cotan.reshape(1, sources * capacity, model_width)
     gate_grads, up_grads, down_grads, partials = ([], [], [], [])
     gate_wgrad, up_wgrad, down_wgrad, gate_grad, up_grad = expert_pass(
         expert_inputs[0], expert_cotan[0], gate_weight[0], up_weight[0], down_weight[0]
@@ -154,18 +444,12 @@
             jnp.bfloat16
         )
     )
-    partial_slots = jnp.swapaxes(
-        jnp.stack(partials).reshape(EXP_DEV, sources, capacity, model_width), 0, 1
-    )
-    partial_slots = partial_slots.reshape(sources * EXP_DEV * capacity, model_width)
-    summed = (
-        lax.psum_scatter(partial_slots, "tp", scatter_dimension=1, tiled=True)
-        .astype(jnp.float32)
-        .astype(jnp.bfloat16)
-    )
-    part_back = lax.all_to_all(summed, "sp", split_axis=0, concat_axis=0, tiled=True)
-    quarter_grad = jnp.sum(
-        part_back[slot_index].reshape(token_count, TOP, column_width).astype(jnp.float32), axis=1
+    part_back, lru_rows = return_rows(
+        sources, partials[0].reshape(sources, capacity, model_width), lru_out
+    )
+    lru_rows = lru_rows.reshape(sources * token_count, lru_out.shape[1])
+    quarter_grad = contract(
+        chosen, part_back.reshape(sources * capacity, column_width), 1, 0
     ).astype(jnp.bfloat16)
     normed_grad = lax.all_gather(quarter_grad, "tp", axis=1, tiled=True).astype(jnp.float32)
     scaled_grad = gain_row * normed_grad
@@ -173,11 +457,6 @@
         scaled_grad - unit_rows * jnp.mean(unit_rows * scaled_grad, axis=1, keepdims=True)
     )
     stream_grad_b = stream_grad.astype(jnp.bfloat16)
-    total_state = states[0] + states[1]
-    gate_float = gate_branch.astype(jnp.float32)
-    gelu_gate, gelu_back = jax.vjp(jax.nn.gelu, gate_float)
-    lru_out = (total_state * gelu_gate).astype(jnp.bfloat16)
-    lru_rows = lax.all_gather(lru_out, "sp", axis=0, tiled=True)
     piece_width = column_width // sources
     own_piece = lax.dynamic_slice_in_dim(
         stream_grad_b.reshape(token_count, sources, quarters, piece_width),
@@ -223,7 +502,7 @@
                 inner_sum,
             )
         )
-    gathered = lax.all_gather(jnp.concatenate(summaries, axis=0), "sp", axis=1, tiled=False)
+    gathered = jnp.swapaxes(share(sources, jnp.concatenate(summaries, axis=0)), 0, 1)
     device_index = lax.axis_index("sp")
     zero_row = jnp.zeros_like(ones_row)
     from_right = linear_scan(gathered[0], gathered[1], True)[1]

time: 413 us -> 320 us (0.77); the launches traced: 408 us -> 319 us
  Pallas kernels: 0 us -> 154 us
  waiting for transfers between devices: 155 us -> 28 us
  blocking collectives: 104 us -> 0 us
  local copies, waits for them, and re-layouts: 47.5 us -> 37.3 us
  matrix products: 43.8 us -> 50.7 us
  starting transfers between devices: 11.4 us -> 5.71 us
    pallas_call x0 -> x3, Pallas kernels: none -> 154 us  [the longest x1 84.1 us: dispatch(): pl.pallas_call(functools.partial(dispatch_kernel, sources), out_shape=(ro...]
    all_to_all x2 -> x0, blocking collectives: 73.2 us -> none  [the longest x1 38.9 us: body(): lax.all_to_all(slot_inputs, 'sp', split_axis=0, concat_axis=0, tiled=True)]
    reduce_scatter x1 -> x0, waiting for transfers between devices: 51.3 us -> none  [body(): lax.psum_scatter(partial_slots, 'tp', scatter_dimension=1, tiled=True)]
    all_gather x3 -> x0, waiting for transfers between devices: 45 us -> none  [the longest x1 32.2 us: body(): lax.all_gather(part_cotan, 'tp', axis=1, tiled=True)]
    all_to_all x1 -> x0, waiting for transfers between devices: 31.2 us -> none  [body(): lax.all_to_all(summed, 'sp', split_axis=0, concat_axis=0, tiled=True)]
    all_gather x1 -> x0, blocking collectives: 30.7 us -> none  [body(): lax.all_gather(jnp.concatenate(summaries, axis=0), 'sp', axis=1, tiled=Fa...]
    gather x4 -> x0, local copies, waits for them, and re-layouts: 11.8 us -> none  [the longest x1 3.47 us: body(): slot_inputs = jnp.concatenate([normed_cols, zero_row])[slot_token]]
    dot_general x10 -> x13, matrix products: 36.4 us -> 45.4 us  [contract(): lax.dot_general(left, right, (((left_dim,), (right_dim,)), ((), ())), pre...]
  transfers between devices with their start and end apart: 8 -> 3, of which waited for: 7 -> 3; matrix products, arithmetic and copies ran while one was open for 13% -> 12% of each run, Pallas kernels for 0% -> 0%
where the time goes in v2:
time: 320 us; the launch traced here: 319 us
  Pallas kernels  154 us (48%)
  matrix products  50.7 us (16%)
  local copies, waits for them, and re-layouts  37.3 us (12%)
  waiting for transfers between devices  28 us (9%)
  other arithmetic  27.3 us (9%)
  between operations  16.3 us (5%)
  starting transfers between devices  5.71 us (2%)
    pallas_call x1, Pallas kernels, dispatch(): pl.pallas_call(functools.partial(dispatch_kernel, sources), out_shape=(ro...  84.1 us
    pallas_call x1, Pallas kernels, return_rows(): pl.pallas_call(functools.partial(return_kernel, sources), out_shape=(jax....  61.7 us
    dot_general x13, matrix products, contract(): lax.dot_general(left, right, (((left_dim,), (right_dim,)), ((), ())), pre...  45.4 us
    all_gather x1, waiting for transfers between devices, body(): lax.all_gather(piece_rows.reshape(sources * token_count, piece_width), 't...  15.1 us
    pad x60, local copies, waits for them, and re-layouts, linear_scan(): lax.associative_scan(combine, (coeffs, values), axis=0, reverse=reverse)  10.5 us
    all_gather x1, waiting for transfers between devices, body(): lax.all_gather(quarter_grad, 'tp', axis=1, tiled=True).astype(jnp.float32)  9.93 us
    slice x132, local copies, waits for them, and re-layouts, linear_scan(): lax.associative_scan(combine, (coeffs, values), axis=0, reverse=reverse)  8.96 us
    pallas_call x1, Pallas kernels, share(): pl.pallas_call(functools.partial(share_kernel, sources), out_shape=jax.Sh...  8.02 us
  transfers between devices with their start and end apart: 3, of which 3 were waited for; matrix products, arithmetic and copies ran while one was open for 12% of the time, Pallas kernels for 0%

profile of v2, /device:TPU:0, one launch (start us, length us, event | category | flops | bytes accessed | tf_op | source)
XLA Modules:
  0.0 319.1 jit_solution(6287228203379916513)
XLA Ops:
  8.5 2.1 fusion.3
  12.8 4.2 %convert_multiply_fusion = f32[256,4096]{1,0:T(8,128)} fusion(bf16[256,4096]{1,0:T(8,128)(2,1)} %param.17, f32[256]{0:T(256)S(1)} %add_rsqrt_fusion), kind=kLoop, calls=%fused_computation.1 | loop fusion | flops 2097152 | bytes 6292480 | tf_op jit(solution)/shard_map/mul | solution.py:403
  16.9 2.7 multiply_convert_fusion
  19.6 2.8 convolution_convert_fusion.3
  22.4 84.1 %shard_map.199 = (bf16[8,80,4096]{2,1,0:T(8,128)(2,1)}, bf16[8,80,4096]{2,1,0:T(8,128)(2,1)}) custom-call(bf16[8,80,1024]{2,1,0:T(8,128)(2,1)} %bitcast.268, bf16[8,80,1024]{2,1,0:T(8,128)(2,1)} %bitcast.273), custom_call_target="tpu_custom_call" | custom-call | tf_op jit(solution)/shard_map/pallas_call | solution.py:217
  106.6 4.2 %fusion.6 = f32[640,256]{1,0:T(8,128)S(1)} fusion(bf16[640,4096]{1,0:T(8,128)(2,1)} %bitcast.304, bf16[1,4096,256]{2,1,0:T(8,128)(2,1)S(1)} %copy-done), kind=kOutput, calls=%fused_computation.16 | convolution fusion | flops 1342177280 | bytes 7995392 | tf_op jit(solution)/shard_map/dot_general | solution.py:20
  110.8 4.3 %fusion.9 = f32[640,256]{1,0:T(8,128)S(1)} fusion(bf16[640,4096]{1,0:T(8,128)(2,1)} %bitcast.305, bf16[1,4096,256]{2,1,0:T(8,128)(2,1)S(1)} %copy-done.6), kind=kOutput, calls=%fused_computation.19 | convolution fusion | flops 1342177280 | bytes 7995392 | tf_op jit(solution)/shard_map/dot_general | solution.py:20
  119.3 3.8 %add_convert_fusion = bf16[640,4096]{1,0:T(8,128)(2,1)} fusion(f32[640,4096]{1,0:T(8,128)S(1)} %fusion.4, bf16[640,256]{1,0:T(8,128)(2,1)S(1)} %get-tuple-element.14, bf16[1,4096,256]{2,1,0:T(8,128)(2,1)S(1)} %copy-done.6), kind=kOutput, calls=%fused_computation | convolution fusion | flops 1347420160 | bytes 18153472 | tf_op jit(solution)/shard_map/dot_general | solution.py:20
  123.1 61.7 %shard_map.200 = (bf16[8,80,1024]{2,1,0:T(8,128)(2,1)}, bf16[8,256,256]{2,1,0:T(8,128)(2,1)}) custom-call(bf16[8,80,4096]{2,1,0:T(8,128)(2,1)} %bitcast.267, bf16[256,256]{1,0:T(8,128)(2,1)} %multiply_convert_fusion.5.lru_ref), custom_call_target="tpu_custom_call" | custom-call | tf_op jit(solution)/shard_map/pallas_call | solution.py:332
  184.8 2.7 convolution_convert_fusion.4
  194.0 5.8 %fusion.1 = bf16[1,4096,256]{2,1,0:T(8,128)(2,1)} fusion(bf16[640,4096]{1,0:T(8,128)(2,1)} %bitcast.306, bf16[640,256]{1,0:T(8,128)(2,1)S(1)} %copy-done.33), kind=kOutput, calls=%fused_computation.7 | convolution fusion | flops 1343225856 | bytes 7667712 | tf_op jit(solution)/shard_map/dot_general | solution.py:20
  199.8 5.9 %fusion = bf16[1,4096,256]{2,1,0:T(8,128)(2,1)} fusion(bf16[640,4096]{1,0:T(8,128)(2,1)} %bitcast.307, bf16[640,256]{1,0:T(8,128)(2,1)S(1)} %copy-done.31), kind=kOutput, calls=%fused_computation.6 | convolution fusion | flops 1343225856 | bytes 7667712 | tf_op jit(solution)/shard_map/dot_general | solution.py:20
  205.8 3.3 %fusion.2 = bf16[1,256,4096]{2,1,0:T(8,128)(2,1)} fusion(bf16[640,4096]{1,0:T(8,128)(2,1)S(1)} %bitcast.303, f32[640,256]{1,0:T(8,128)S(1)} %copy-done.57, f32[640,256]{1,0:T(8,128)S(1)} %copy-done.55), kind=kOutput, calls=%fused_computation.8 | convolution fusion | flops 1344208896 | bytes 8650752 | tf_op jit(solution)/shard_map/dot_general | solution.py:20
  209.0 9.9 %all-gather.3.cloned.1.call-done = bf16[256,4096]{1,0:T(8,128)(2,1)} async-done(((bf16[256,1024]{1,0:T(8,128)(2,1)}), bf16[256,4096]{1,0:T(8,128)(2,1)}) %all-gather.3.cloned.1.call-update) | async-done | bytes 2097168 | tf_op jit(solution)/shard_map/all_gather | solution.py:454
  219.0 2.7 multiply_reduce_fusion
  221.8 3.0 add_convert_fusion.1
  224.9 4.6 %reshape.186 = bf16[256,8,4,128]{3,2,1,0:T(4,128)(2,1)} reshape(bf16[256,4096]{1,0:T(8,128)(2,1)} %add_convert_fusion.1) | data formatting | bytes 4194304 | tf_op jit(solution)/shard_map/reshape | solution.py:462
  229.4 3.2 %fusion.38 = (f32[256,256]{1,0:T(8,128)}, f32[256,256]{1,0:T(8,128)S(1)}) fusion(bf16[256,256]{1,0:T(8,128)(2,1)} %param.26, f32[2,256,256]{2,1,0:T(8,128)} %param.31, bf16[256,4096]{1,0:T(8,128)(2,1)S(1)} %copy-done.3, bf16[4096,256]{1,0:T(8,128)(2,1)} %param.24), kind=kOutput, calls=%fused_computation.78 | convolution fusion | flops 538443776 | bytes 5373952 | tf_op jit(solution)/shard_map/dot_general | solution.py:20
  256.1 8.0 %shard_map.201 = f32[8,4,256]{2,1,0:T(4,128)} custom-call(f32[4,256]{1,0:T(4,128)} %pad_maximum_fusion.22.own_ref), custom_call_target="tpu_custom_call" | custom-call | tf_op jit(solution)/shard_map/pallas_call | solution.py:368
  267.6 5.6 %all-to-all-start = ((bf16[8,256,128]{2,1,0:T(8,128)(2,1)}), bf16[8,256,128]{2,1,0:T(8,128)(2,1)S(1)}, u32[]{:S(2)}, u32[]{:S(2)}) async-start(bf16[8,256,128]{2,1,0:T(8,128)(2,1)} %bitcast.261), calls=%async_computation | async-start | bytes 1048576 | tf_op jit(solution)/shard_map/all_to_all | solution.py:467
  284.0 3.0 all-to-all-done
  289.2 1.9 convolution_add_fusion.1
  293.8 15.1 %all-gather.5.cloned.1.call-done = bf16[2048,512]{1,0:T(8,128)(2,1)} async-done(((bf16[2048,128]{1,0:T(8,128)(2,1)}), bf16[2048,512]{1,0:T(8,128)(2,1)}) %all-gather.5.cloned.1.call-update) | async-done | bytes 2097168 | tf_op jit(solution)/shard_map/all_gather | solution.py:468
  308.9 3.4 %fusion.179 = f32[512,256]{1,0:T(8,128)} fusion(bf16[2048,512]{1,0:T(8,128)(2,1)} %all-gather.5.cloned.1.call-done, bf16[2048,256]{1,0:T(8,128)(2,1)} %bitcast.274), kind=kOutput, calls=%fused_computation.357 | convolution fusion | flops 536870912 | bytes 3670016 | tf_op jit(solution)/shard_map/dot_general | solution.py:20
  (486 shorter events, 54.9 us)
Async XLA Ops:
  7.2 99.4 %copy-start = (bf16[1,4096,256]{2,1,0:T(8,128)(2,1)S(1)}, bf16[1,4096,256]{2,1,0:T(8,128)(2,1)}, u32[]{:S(2)}) copy-start(bf16[1,4096,256]{2,1,0:T(8,128)(2,1)} %param.21) | copy-start | bytes 6291460
  7.2 211.8 %all-gather.3.cloned.1.call-start = ((), (), s32[]{:S(2)}) async-start(), calls=%async_computation.1 | async-start | bytes 2621440 | tf_op jit(solution)/shard_map/all_gather | solution.py:454
  106.6 8.5 %slice-start = ((s8[5242880]{0:T(1024)(128)(4,1)}), s8[4194304]{0:T(1024)(128)(4,1)S(1)}, s32[]{:S(2)}) async-start(s8[5242880]{0:T(1024)(128)(4,1)} %bitcast.298), calls=%async_computation.3 | async-start | bytes 8388608
  194.0 11.7 %slice-start.2 = ((s8[5242880]{0:T(1024)(128)(4,1)}), s8[4194304]{0:T(1024)(128)(4,1)S(1)}, s32[]{:S(2)}) async-start(s8[5242880]{0:T(1024)(128)(4,1)} %bitcast.301), calls=%async_computation.5 | async-start | bytes 8388608
  199.8 5.9 %copy-start.55 = (f32[640,256]{1,0:T(8,128)S(1)}, f32[640,256]{1,0:T(8,128)}, u32[]{:S(2)}) copy-start(f32[640,256]{1,0:T(8,128)} %copy-done.54) | copy-start | bytes 1966084
  199.8 5.9 %copy-start.57 = (f32[640,256]{1,0:T(8,128)S(1)}, f32[640,256]{1,0:T(8,128)}, u32[]{:S(2)}) copy-start(f32[640,256]{1,0:T(8,128)} %copy-done.56) | copy-start | bytes 1966084
  205.7 13.2 %copy-start.2 = (bf16[256,4096]{1,0:T(8,128)(2,1)S(1)}, bf16[256,4096]{1,0:T(8,128)(2,1)}, u32[]{:S(2)}) copy-start(bf16[256,4096]{1,0:T(8,128)(2,1)} %param.17) | copy-start | bytes 6291460
  238.2 6.1 %copy-start.27 = (f32[127,256]{1,0:T(8,128)S(1)}, f32[127,256]{1,0:T(8,128)}, u32[]{:S(2)}) copy-start(f32[127,256]{1,0:T(8,128)} %slice.845) | copy-start | bytes 390148
  245.0 20.4 %copy-start.5 = (bf16[256,8,4,128]{3,2,1,0:T(4,128)(2,1)S(1)}, bf16[256,8,4,128]{3,2,1,0:T(4,128)(2,1)}, u32[]{:S(2)}) copy-start(bf16[256,8,4,128]{3,2,1,0:T(4,128)(2,1)} %reshape.186) | copy-start | bytes 6291460
  246.3 6.8 %copy-start.26 = (f32[128,256]{1,0:T(8,128)S(1)}, f32[128,256]{1,0:T(8,128)}, u32[]{:S(2)}) copy-start(f32[128,256]{1,0:T(8,128)} %concatenate.133) | copy-start | bytes 393220
  252.1 15.4 %copy-start.14 = (f32[256,256]{1,0:T(8,128)}, f32[256,256]{1,0:T(8,128)S(1)}, u32[]{:S(2)}) copy-start(f32[256,256]{1,0:T(8,128)S(1)} %pad.254) | copy-start | bytes 786436
  253.2 14.4 %copy-start.16 = (f32[256,256]{1,0:T(8,128)}, f32[256,256]{1,0:T(8,128)S(1)}, u32[]{:S(2)}) copy-start(f32[256,256]{1,0:T(8,128)S(1)} %pad.270) | copy-start | bytes 786436
  266.5 7.8 %copy-start.13 = (f32[256,256]{1,0:T(8,128)S(1)}, f32[256,256]{1,0:T(8,128)}, u32[]{:S(2)}) copy-start(f32[256,256]{1,0:T(8,128)} %pad.271) | copy-start | bytes 786436
  266.5 9.5 %copy-start.12 = (f32[256,256]{1,0:T(8,128)S(1)}, f32[256,256]{1,0:T(8,128)}, u32[]{:S(2)}) copy-start(f32[256,256]{1,0:T(8,128)} %pad.255) | copy-start | bytes 786436
  267.5 8.5 %copy-start.15 = (f32[256,256]{1,0:T(8,128)S(1)}, f32[256,256]{1,0:T(8,128)}, u32[]{:S(2)}) copy-start(f32[256,256]{1,0:T(8,128)} %copy-done.14) | copy-start | bytes 786436
  267.5 21.5 %copy-start.18 = (f32[256,256]{1,0:T(8,128)S(1)}, f32[256,256]{1,0:T(8,128)}, u32[]{:S(2)}) copy-start(f32[256,256]{1,0:T(8,128)} %pad.303) | copy-start | bytes 786436
  267.5 21.5 %copy-start.19 = (f32[256,256]{1,0:T(8,128)S(1)}, f32[256,256]{1,0:T(8,128)}, u32[]{:S(2)}) copy-start(f32[256,256]{1,0:T(8,128)} %pad.287) | copy-start | bytes 786436
  267.5 21.5 %copy-start.20 = (f32[256,256]{1,0:T(8,128)S(1)}, f32[256,256]{1,0:T(8,128)}, u32[]{:S(2)}) copy-start(f32[256,256]{1,0:T(8,128)} %pad.302) | copy-start | bytes 786436
  267.5 21.5 %copy-start.21 = (f32[256,256]{1,0:T(8,128)S(1)}, f32[256,256]{1,0:T(8,128)}, u32[]{:S(2)}) copy-start(f32[256,256]{1,0:T(8,128)} %pad.286) | copy-start | bytes 786436
  267.6 19.4 %all-to-all-start = ((bf16[8,256,128]{2,1,0:T(8,128)(2,1)}), bf16[8,256,128]{2,1,0:T(8,128)(2,1)S(1)}, u32[]{:S(2)}, u32[]{:S(2)}) async-start(bf16[8,256,128]{2,1,0:T(8,128)(2,1)} %bitcast.261), calls=%async_computation | async-start | bytes 1048576 | tf_op jit(solution)/shard_map/all_to_all | solution.py:467
  273.2 35.7 %all-gather.5.cloned.1.call-start = ((), (), s32[]{:S(2)}) async-start(), calls=%async_computation.2 | async-start | bytes 2621440 | tf_op jit(solution)/shard_map/all_gather | solution.py:468
  276.0 13.2 %copy-start.10 = (f32[2,256,256]{2,1,0:T(8,128)S(1)}, f32[2,256,256]{2,1,0:T(8,128)}, u32[]{:S(2)}) copy-start(f32[2,256,256]{2,1,0:T(8,128)} %param.30) | copy-start | bytes 1572868
  276.0 13.2 %copy-start.29 = (bf16[256,256]{1,0:T(8,128)(2,1)S(1)}, bf16[256,256]{1,0:T(8,128)(2,1)}, u32[]{:S(2)}) copy-start(bf16[256,256]{1,0:T(8,128)(2,1)} %param.25) | copy-start | bytes 393220
  292.6 19.7 %copy-start.1 = (bf16[1,4096,256]{2,1,0:T(8,128)(2,1)S(1)}, bf16[1,4096,256]{2,1,0:T(8,128)(2,1)}, u32[]{:S(2)}) copy-start(bf16[1,4096,256]{2,1,0:T(8,128)(2,1)} %param.21) | copy-start | bytes 6291460
  (41 other events, 109.7 us)
Sparse Core Ops, SparseCore 0:
  187.7 31.2 all-gather.2
  287.9 20.9 all-gather.4
